TPU v7x, 32 devices: a whole 2x2x4 slice. The times are simulated.
32 devices in a mesh: ep: 8 (over z, core), tp: 4 (over y, x).
Axes of the slice: x: 2, y: 2, z: 4, core: 2. Of those that a mesh axis runs over, the one named last changes fastest.
Arguments:
- tokens: bfloat16 [2048, 2048], P('ep'), may hold values from -6 to 6
- norm_gain: float32 [2048], replicated, may hold values from 0.1 to 1.9
- route_ids: int32 [2048, 4], P('ep'), may hold values from 0 to 15, all different within a row; in each aligned block of 256 rows (0 to 255, 256 to 511, ...) at most 96 rows name the same one
- route_weights: float32 [2048, 4], P('ep'), may hold values from 0.1 to 1
- w_gate: bfloat16 [16, 2048, 2048], P('ep', None, 'tp'), may hold values from -0.33007812 to 0.33007812
- w_up: bfloat16 [16, 2048, 2048], P('ep', None, 'tp'), may hold values from -0.33007812 to 0.33007812
- w_down: bfloat16 [16, 2048, 2048], P('ep', None, 'tp'), may hold values from -0.026489258 to 0.026489258
Outputs:
- mixed_out: bfloat16 [2048, 2048], P('ep', 'tp')
Inputs may be any that keep to these rules, and one draw needn't show every extreme that they name: `route_ids`: each token names 4 different experts. Within the tokens of one index of ep (aligned blocks of 256 tokens) no expert is named more than 96 times, a bound that some block reaches.
All inputs are finite; a program needn't handle non-finite values.
Results may differ from a plain program's by a relative error of at most 0.007.
Values may be sent and summed in bfloat16 or wider, within the bound.
A program may use at most 64 MiB of HBM per device.

v0:
```python
import jax
import jax.numpy as jnp
from jax import lax
from jax.sharding import PartitionSpec as P

swiglu_limit = 7.0
swiglu_alpha = 1.702
norm_eps = 1e-05


def clamped_units(gate_pre, up_pre):
    capped = jnp.minimum(gate_pre, swiglu_limit)
    linear = jnp.clip(up_pre, -swiglu_limit, swiglu_limit)
    return capped * jax.nn.sigmoid(swiglu_alpha * capped) * (linear + 1.0)


def expert_work(outgoing, gate_weight, up_weight, down_weight):
    received = lax.all_to_all(outgoing, "ep", split_axis=1, concat_axis=1, tiled=True)
    local_count, sources, capacity, columns = received.shape
    row_count = sources * capacity
    row_block = received.reshape(local_count, row_count, columns)
    shard_piece = lax.all_gather(row_block, "tp", axis=2, tiled=True)
    gate_sum = jnp.einsum(
        "lrd,ldf->lrf", shard_piece, gate_weight, preferred_element_type=jnp.float32
    )
    up_sum = jnp.einsum("lrd,ldf->lrf", shard_piece, up_weight, preferred_element_type=jnp.float32)
    activation = clamped_units(gate_sum, up_sum).astype(jnp.bfloat16)
    out_cols = down_weight.shape[2]
    result = jnp.einsum(
        "lrf,lfd->lrd",
        lax.all_gather(activation, "tp", axis=2, tiled=True),
        down_weight,
        preferred_element_type=jnp.float32,
    )
    result = result.astype(jnp.bfloat16).reshape(local_count, sources, capacity, out_cols)
    return lax.all_to_all(result, "ep", split_axis=1, concat_axis=1, tiled=True)


def per_device(tokens, norm_gain, route_ids, route_weights, w_gate, w_up, w_down):
    local_count = w_gate.shape[0]
    sources = lax.axis_size("ep")
    tp_count = lax.axis_size("tp")
    width = tokens.shape[1]
    columns = width // tp_count
    experts = local_count * sources
    tok_rows, top_count = route_ids.shape
    capacity = 3 * tok_rows * top_count // (2 * experts)
    values = tokens.astype(jnp.float32)
    row_mean = jnp.mean(values, axis=1, keepdims=True)
    centred = values - row_mean
    row_var = jnp.mean(centred * centred, axis=1, keepdims=True)
    offset = lax.axis_index("tp") * columns
    own_cols = lax.dynamic_slice_in_dim(centred, offset, columns, 1)
    own_gain = lax.dynamic_slice_in_dim(norm_gain, offset, columns, 0)
    normed = (own_cols * lax.rsqrt(row_var + norm_eps) * own_gain).astype(jnp.bfloat16)
    flat_ids = route_ids.reshape(-1)
    matches = (flat_ids[:, None] == jnp.arange(experts, dtype=jnp.int32)[None, :]).astype(jnp.int32)
    earlier = jnp.cumsum(matches, axis=0) - matches
    slot_index = jnp.sum(earlier * matches, axis=1)
    position = (
        flat_ids % local_count * (sources * capacity)
        + flat_ids // local_count * capacity
        + slot_index
    )
    buffer_rows = local_count * sources * capacity
    placed = (
        position.reshape(tok_rows, top_count)[:, :, None]
        == jnp.arange(buffer_rows, dtype=jnp.int32)[None, None, :]
    )
    placement_matrix = jnp.any(placed, axis=1).astype(jnp.bfloat16)
    outgoing = jnp.einsum("tp,td->pd", placement_matrix, normed, preferred_element_type=jnp.float32)
    outgoing = outgoing.astype(jnp.bfloat16).reshape(local_count, sources, capacity, columns)
    returned = jnp.concatenate(
        [
            expert_work(
                outgoing[number : number + 1],
                w_gate[number : number + 1],
                w_up[number : number + 1],
                w_down[number : number + 1],
            )
            for number in range(local_count)
        ],
        axis=0,
    )
    flat_out = returned.reshape(buffer_rows, columns)
    picked = flat_out[position].reshape(tok_rows, top_count, columns).astype(jnp.float32)
    return jnp.sum(picked * route_weights[:, :, None], axis=1).astype(jnp.bfloat16)


def solution(mesh):
    return jax.shard_map(
        per_device,
        mesh=mesh,
        in_specs=(
            P("ep", None),
            P(),
            P("ep", None),
            P("ep", None),
            P("ep", None, "tp"),
            P("ep", None, "tp"),
            P("ep", None, "tp"),
        ),
        out_specs=P("ep", "tp"),
        check_vma=False,
    )
```

profile of v0, /device:TPU:0, one launch (start us, length us, event | category | flops | bytes accessed | tf_op | source)
XLA Modules:
  0.0 269.5 jit_solution(14024327743090888040)
XLA Ops:
  6.5 0.9 copy.62
  7.7 4.5 %reduce-window.6 = s32[16,8,128]{2,1,0:T(8,128)S(1)} reduce-window(s32[16,8,128]{2,1,0:T(8,128)S(1)} %fusion.42, s32[]{:T(128)} %constant.28.clone.1), window={size=1x1x128 pad=0_0x0_0x127_0}, to_apply=%region_0.0 | reduce-window | flops 2080768 | bytes 131076 | tf_op jit(solution)/shard_map/reduce-window
  12.9 0.7 fusion.45
  13.6 1.7 fusion
  16.0 0.8 dynamic_slice.7
  16.8 1.7 convolution_convert_fusion
  18.6 27.2 %all_to_all.20 = bf16[1,8,96,512]{3,2,0,1:T(8,128)(2,1)} all-to-all(bf16[1,8,96,512]{3,2,0,1:T(8,128)(2,1)S(1)} %bitcast.82), channel_id=1, replica_groups=mesh['ep'=8,'tp'=4] {'ep'}, dimensions={1} | all-to-all | bytes 1572864 | tf_op jit(solution)/shard_map/all_to_all | solution.py:18
  45.9 24.0 %all_to_all.21 = bf16[1,8,96,512]{3,2,0,1:T(8,128)(2,1)} all-to-all(bf16[1,8,96,512]{3,2,0,1:T(8,128)(2,1)S(1)} %bitcast.81), channel_id=1, replica_groups=mesh['ep'=8,'tp'=4] {'ep'}, dimensions={1} | all-to-all | bytes 1572864 | tf_op jit(solution)/shard_map/all_to_all | solution.py:18
  70.0 18.6 %all-gather.7.cloned.1.call-done = bf16[1,768,2048]{2,1,0:T(8,128)(2,1)} async-done(((bf16[1,768,512]{2,1,0:T(8,128)(2,1)}), bf16[1,768,2048]{2,1,0:T(8,128)(2,1)}) %all-gather.7.cloned.1.call-update) | async-done | bytes 3145744 | tf_op jit(solution)/shard_map/all_gather | solution.py:22
  88.6 4.5 %fusion.7 = f32[768,512]{1,0:T(8,128)S(1)} fusion(bf16[1,768,2048]{2,1,0:T(8,128)(2,1)} %all-gather.7.cloned.1.call-done, bf16[2,2048,512]{2,1,0:T(8,128)(2,1)} %param.11), kind=kOutput, calls=%fused_computation.9 | convolution fusion | flops 1610612736 | bytes 6815744 | tf_op jit(solution)/shard_map/lrd,ldf->lrf/dot_general | solution.py:23
  93.3 3.0 %multiply_convert_fusion.1 = bf16[768,512]{1,0:T(8,128)(2,1)} fusion(f32[768,512]{1,0:T(8,128)S(1)} %fusion.7, bf16[2,2048,512]{2,1,0:T(8,128)(2,1)S(1)} %copy-done.2, bf16[1,768,2048]{2,1,0:T(8,128)(2,1)S(1)} %copy-done.5), kind=kOutput, calls=%fused_computation.32 | convolution fusion | flops 1614544896 | bytes 7602176 | tf_op jit(solution)/shard_map/lrd,ldf->lrf/dot_general | solution.py:26
  96.4 37.8 %all-gather.9.cloned.1.call-done = bf16[1,768,2048]{2,1,0:T(8,128)(2,1)} async-done(((bf16[1,768,512]{2,1,0:T(8,128)(2,1)}), bf16[1,768,2048]{2,1,0:T(8,128)(2,1)}) %all-gather.9.cloned.1.call-update) | async-done | bytes 3145744 | tf_op jit(solution)/shard_map/all_gather | solution.py:22
  134.2 4.5 %fusion.3 = f32[768,512]{1,0:T(8,128)S(1)} fusion(bf16[1,768,2048]{2,1,0:T(8,128)(2,1)} %all-gather.9.cloned.1.call-done, bf16[2,2048,512]{2,1,0:T(8,128)(2,1)} %param.11), kind=kOutput, calls=%fused_computation.5 | convolution fusion | flops 1610612736 | bytes 6815744 | tf_op jit(solution)/shard_map/lrd,ldf->lrf/dot_general | solution.py:23
  138.9 3.0 %multiply_convert_fusion = bf16[768,512]{1,0:T(8,128)(2,1)} fusion(f32[768,512]{1,0:T(8,128)S(1)} %fusion.3, bf16[2,2048,512]{2,1,0:T(8,128)(2,1)S(1)} %copy-done.3, bf16[1,768,2048]{2,1,0:T(8,128)(2,1)S(1)} %copy-done.4), kind=kOutput, calls=%fused_computation.31 | convolution fusion | flops 1614544896 | bytes 7602176 | tf_op jit(solution)/shard_map/lrd,ldf->lrf/dot_general | solution.py:26
  141.9 37.8 %all-gather.11.cloned.1.call-done = bf16[768,2048]{1,0:T(8,128)(2,1)} async-done(((bf16[768,512]{1,0:T(8,128)(2,1)}), bf16[768,2048]{1,0:T(8,128)(2,1)}) %all-gather.11.cloned.1.call-update) | async-done | bytes 3145744 | tf_op jit(solution)/shard_map/all_gather | solution.py:31
  179.8 5.2 %fusion.31 = bf16[768,512]{1,0:T(8,128)(2,1)} fusion(bf16[768,2048]{1,0:T(8,128)(2,1)} %all-gather.11.cloned.1.call-done, bf16[2,2048,512]{2,1,0:T(8,128)(2,1)} %param.13), kind=kOutput, calls=%fused_computation.33 | convolution fusion | flops 1611005952 | bytes 6029312 | tf_op jit(solution)/shard_map/lrf,lfd->lrd/dot_general | solution.py:29
  185.0 4.6 %all-to-all-start.1 = ((bf16[1,8,96,512]{3,2,0,1:T(8,128)(2,1)}), bf16[1,8,96,512]{3,2,0,1:T(8,128)(2,1)S(1)}, u32[]{:S(2)}, u32[]{:S(2)}) async-start(bf16[1,8,96,512]{3,2,0,1:T(8,128)(2,1)} %bitcast.10), calls=%async_computation.1 | async-start | bytes 1572864 | tf_op jit(solution)/shard_map/all_to_all | solution.py:36
  189.6 35.6 %all-gather.13.cloned.1.call-done = bf16[768,2048]{1,0:T(8,128)(2,1)} async-done(((bf16[768,512]{1,0:T(8,128)(2,1)}), bf16[768,2048]{1,0:T(8,128)(2,1)}) %all-gather.13.cloned.1.call-update) | async-done | bytes 3145744 | tf_op jit(solution)/shard_map/all_gather | solution.py:31
  225.2 5.2 %fusion.34 = bf16[768,512]{1,0:T(8,128)(2,1)} fusion(bf16[768,2048]{1,0:T(8,128)(2,1)} %all-gather.13.cloned.1.call-done, bf16[2,2048,512]{2,1,0:T(8,128)(2,1)} %param.13), kind=kOutput, calls=%fused_computation.34 | convolution fusion | flops 1611005952 | bytes 6029312 | tf_op jit(solution)/shard_map/lrf,lfd->lrd/dot_general | solution.py:29
  230.4 4.6 %all-to-all-start.3 = ((bf16[1,8,96,512]{3,2,0,1:T(8,128)(2,1)}), bf16[1,8,96,512]{3,2,0,1:T(8,128)(2,1)S(1)}, u32[]{:S(2)}, u32[]{:S(2)}) async-start(bf16[1,8,96,512]{3,2,0,1:T(8,128)(2,1)} %bitcast.19), calls=%async_computation.3 | async-start | bytes 1572864 | tf_op jit(solution)/shard_map/all_to_all | solution.py:36
  235.3 20.6 %all-to-all-done.3 = bf16[1,8,96,512]{3,2,0,1:T(8,128)(2,1)S(1)} async-done(((bf16[1,8,96,512]{3,2,0,1:T(8,128)(2,1)}), bf16[1,8,96,512]{3,2,0,1:T(8,128)(2,1)S(1)}, u32[]{:S(2)}, u32[]{:S(2)}) %all-to-all-start.3) | async-done | bytes 786464 | tf_op jit(solution)/shard_map/all_to_all | solution.py:36
  256.2 4.0 %gather_fusion = bf16[1024,512]{1,0:T(8,128)(2,1)S(1)} fusion(bf16[1536,512]{1,0:T(8,128)(2,1)S(1)} %bitcast.78, s32[1024]{0:T(1024)S(1)} %broadcast_clamp_fusion), kind=kCustom, calls=%fused_computation | custom fusion | bytes 2101248 | tf_op jit(solution)/shard_map/gather | solution.py:86
  260.2 0.7 reshape.290
  260.9 2.1 multiply_reduce_fusion
  (44 shorter events, 2.9 us)
Async XLA Ops:
  6.5 8.8 %copy-start = (bf16[256,2048]{1,0:T(8,128)(2,1)S(1)}, bf16[256,2048]{1,0:T(8,128)(2,1)}, u32[]{:S(2)}) copy-start(bf16[256,2048]{1,0:T(8,128)(2,1)} %param.7) | copy-start | bytes 3145732
  6.5 82.1 %all-gather.7.cloned.1.call-start = ((), (), s32[]{:S(2)}) async-start(), calls=%async_computation.4 | async-start | bytes 3932160 | tf_op jit(solution)/shard_map/all_gather | solution.py:22
  45.8 88.4 %all-gather.9.cloned.1.call-start = ((), (), s32[]{:S(2)}) async-start(), calls=%async_computation.5 | async-start | bytes 3932160 | tf_op jit(solution)/shard_map/all_gather | solution.py:22
  69.9 109.8 %all-gather.11.cloned.1.call-start = ((), (), s32[]{:S(2)}) async-start(), calls=%async_computation.6 | async-start | bytes 3932160 | tf_op jit(solution)/shard_map/all_gather | solution.py:31
  88.6 4.5 %copy-start.2 = (bf16[2,2048,512]{2,1,0:T(8,128)(2,1)S(1)}, bf16[2,2048,512]{2,1,0:T(8,128)(2,1)}, u32[]{:S(2)}) copy-start(bf16[2,2048,512]{2,1,0:T(8,128)(2,1)} %param.12) | copy-start | bytes 12582916
  88.6 4.7 %copy-start.5 = (bf16[1,768,2048]{2,1,0:T(8,128)(2,1)S(1)}, bf16[1,768,2048]{2,1,0:T(8,128)(2,1)}, u32[]{:S(2)}) copy-start(bf16[1,768,2048]{2,1,0:T(8,128)(2,1)} %all-gather.7.cloned.1.call-done) | copy-start | bytes 9437188
  96.4 128.8 %all-gather.13.cloned.1.call-start = ((), (), s32[]{:S(2)}) async-start(), calls=%async_computation.7 | async-start | bytes 3932160 | tf_op jit(solution)/shard_map/all_gather | solution.py:31
  134.2 4.5 %copy-start.3 = (bf16[2,2048,512]{2,1,0:T(8,128)(2,1)S(1)}, bf16[2,2048,512]{2,1,0:T(8,128)(2,1)}, u32[]{:S(2)}) copy-start(bf16[2,2048,512]{2,1,0:T(8,128)(2,1)} %param.12) | copy-start | bytes 12582916
  134.2 4.7 %copy-start.4 = (bf16[1,768,2048]{2,1,0:T(8,128)(2,1)S(1)}, bf16[1,768,2048]{2,1,0:T(8,128)(2,1)}, u32[]{:S(2)}) copy-start(bf16[1,768,2048]{2,1,0:T(8,128)(2,1)} %all-gather.9.cloned.1.call-done) | copy-start | bytes 9437188
  185.0 45.4 %all-to-all-start.1 = ((bf16[1,8,96,512]{3,2,0,1:T(8,128)(2,1)}), bf16[1,8,96,512]{3,2,0,1:T(8,128)(2,1)S(1)}, u32[]{:S(2)}, u32[]{:S(2)}) async-start(bf16[1,8,96,512]{3,2,0,1:T(8,128)(2,1)} %bitcast.10), calls=%async_computation.1 | async-start | bytes 1572864 | tf_op jit(solution)/shard_map/all_to_all | solution.py:36
  189.6 45.5 %copy-start.1 = (f32[256,4]{0,1:T(4,128)S(1)}, f32[256,4]{0,1:T(4,128)}, u32[]{:S(2)}) copy-start(f32[256,4]{0,1:T(4,128)} %param.10) | copy-start | bytes 12292
  230.4 25.6 %all-to-all-start.3 = ((bf16[1,8,96,512]{3,2,0,1:T(8,128)(2,1)}), bf16[1,8,96,512]{3,2,0,1:T(8,128)(2,1)S(1)}, u32[]{:S(2)}, u32[]{:S(2)}) async-start(bf16[1,8,96,512]{3,2,0,1:T(8,128)(2,1)} %bitcast.19), calls=%async_computation.3 | async-start | bytes 1572864 | tf_op jit(solution)/shard_map/all_to_all | solution.py:36
Sparse Core Ops, SparseCore 0:
  45.9 42.6 all-gather.6
  90.4 43.6 all-gather.8
  136.0 43.6 all-gather.10
  181.4 43.6 all-gather.12
where the time goes:
time: 270 us; the launch traced here: 269 us
  waiting for transfers between devices  150 us (56%)
  blocking collectives  51.2 us (19%)
  matrix products  27 us (10%)
  between operations  13.3 us (5%)
  other arithmetic  10 us (4%)
  starting transfers between devices  9.36 us (3%)
  local copies, waits for them, and re-layouts  8.03 us (3%)
    all_gather x2, waiting for transfers between devices, expert_work(): lax.all_gather(activation, 'tp', axis=2, tiled=True)  73.4 us
    all_gather x2, waiting for transfers between devices, expert_work(): shard_piece = lax.all_gather(row_block, 'tp', axis=2, tiled=True)  56.4 us
    all_to_all x2, blocking collectives, expert_work(): lax.all_to_all(outgoing, 'ep', split_axis=1, concat_axis=1, tiled=True)  51.2 us
    all_to_all x2, waiting for transfers between devices, expert_work(): return lax.all_to_all(result, 'ep', split_axis=1, concat_axis=1, tiled=True)  20.6 us
    dot_general x2, matrix products, expert_work(): jnp.einsum('lrf,lfd->lrd', lax.all_gather(activation, 'tp', axis=2, tiled...  10.4 us
    all_to_all x2, starting transfers between devices, expert_work(): return lax.all_to_all(result, 'ep', split_axis=1, concat_axis=1, tiled=True)  9.23 us
    dot_general x2, matrix products, expert_work(): jnp.einsum('lrd,ldf->lrf', shard_piece, gate_weight, preferred_element_ty...  8.95 us
    dot_general x2, matrix products, expert_work(): jnp.einsum('lrd,ldf->lrf', shard_piece, up_weight, preferred_element_type...  5.99 us
  transfers between devices with their start and end apart: 6, of which 5 were waited for; matrix products, arithmetic and copies ran while one was open for 10% of the time, Pallas kernels for 0%

commit v1 on v0

--- a/solution.py
+++ b/solution.py
@@ -26,12 +26,27 @@
     up_sum = jnp.einsum("lrd,ldf->lrf", shard_piece, up_weight, preferred_element_type=jnp.float32)
     activation = clamped_units(gate_sum, up_sum).astype(jnp.bfloat16)
     out_cols = down_weight.shape[2]
-    result = jnp.einsum(
+    size, mine = (lax.axis_size("tp"), lax.axis_index("tp"))
+    left = [(i, (i - 1) % size) for i in range(size)]
+    rows = activation.shape[2]
+    carried = activation
+    so_far = jnp.einsum(
         "lrf,lfd->lrd",
-        lax.all_gather(activation, "tp", axis=2, tiled=True),
-        down_weight,
+        carried,
+        lax.dynamic_slice_in_dim(down_weight, mine * rows, carried.shape[2], axis=1),
         preferred_element_type=jnp.float32,
     )
+    for hop in range(1, size):
+        carried = lax.ppermute(carried, "tp", left)
+        so_far = so_far + jnp.einsum(
+            "lrf,lfd->lrd",
+            carried,
+            lax.dynamic_slice_in_dim(
+                down_weight, (mine + hop) % size * rows, carried.shape[2], axis=1
+            ),
+            preferred_element_type=jnp.float32,
+        )
+    result = so_far
     result = result.astype(jnp.bfloat16).reshape(local_count, sources, capacity, out_cols)
     return lax.all_to_all(result, "ep", split_axis=1, concat_axis=1, tiled=True)
 

time: 270 us -> 284 us (1.052)
  starting transfers between devices: 9.36 us -> 21 us
  waiting for transfers between devices: 150 us -> 154 us
    all_gather x2 -> x0, waiting for transfers between devices: 73.4 us -> none  [expert_work(): lax.all_gather(activation, 'tp', axis=2, tiled=True)]
    ppermute x0 -> x6, waiting for transfers between devices: none -> 63.4 us  [expert_work(): carried = lax.ppermute(carried, 'tp', left)]
    all_gather x2, waiting for transfers between devices: 56.4 us -> 70.4 us  [expert_work(): shard_piece = lax.all_gather(row_block, 'tp', axis=2, tiled=True)]
    ppermute x0 -> x6, starting transfers between devices: none -> 11.6 us  [expert_work(): carried = lax.ppermute(carried, 'tp', left)]
    dot_general x2 -> x8, matrix products: 10.4 us -> 9.75 us  [expert_work(): jnp.einsum('lrf,lfd->lrd', carried, lax.dynamic_slice_in_dim(down_weight,...]
  transfers between devices with their start and end apart: 6 -> 10, of which waited for: 5 -> 8; matrix products, arithmetic and copies ran while one was open for 10% -> 8% of each run, Pallas kernels for 0% -> 0%
where the time goes in v1:
time: 284 us; the launch traced here: 283 us
  waiting for transfers between devices  154 us (54%)
  blocking collectives  51.3 us (18%)
  matrix products  24.6 us (9%)
  starting transfers between devices  21 us (7%)
  between operations  13.6 us (5%)
  other arithmetic  10 us (4%)
  local copies, waits for them, and re-layouts  8.09 us (3%)
    all_gather x2, waiting for transfers between devices, expert_work(): shard_piece = lax.all_gather(row_block, 'tp', axis=2, tiled=True)  70.4 us
    ppermute x6, waiting for transfers between devices, expert_work(): carried = lax.ppermute(carried, 'tp', left)  63.4 us
    all_to_all x2, blocking collectives, expert_work(): lax.all_to_all(outgoing, 'ep', split_axis=1, concat_axis=1, tiled=True)  51.3 us
    all_to_all x2, waiting for transfers between devices, expert_work(): return lax.all_to_all(result, 'ep', split_axis=1, concat_axis=1, tiled=True)  20.6 us
    ppermute x6, starting transfers between devices, expert_work(): carried = lax.ppermute(carried, 'tp', left)  11.6 us
    dot_general x8, matrix products, expert_work(): jnp.einsum('lrf,lfd->lrd', carried, lax.dynamic_slice_in_dim(down_weight,...  9.75 us
    all_to_all x2, starting transfers between devices, expert_work(): return lax.all_to_all(result, 'ep', split_axis=1, concat_axis=1, tiled=True)  9.35 us
    dot_general x2, matrix products, expert_work(): jnp.einsum('lrd,ldf->lrf', shard_piece, gate_weight, preferred_element_ty...  8.93 us
  transfers between devices with their start and end apart: 10, of which 8 were waited for; matrix products, arithmetic and copies ran while one was open for 8% of the time, Pallas kernels for 0%

profile of v1, /device:TPU:0, one launch (start us, length us, event | category | flops | bytes accessed | tf_op | source)
XLA Modules:
  0.0 283.1 jit_solution(9522714354775366519)
XLA Ops:
  7.7 4.5 %reduce-window.6 = s32[16,8,128]{2,1,0:T(8,128)S(1)} reduce-window(s32[16,8,128]{2,1,0:T(8,128)S(1)} %fusion.58, s32[]{:T(128)} %constant.75.clone.1), window={size=1x1x128 pad=0_0x0_0x127_0}, to_apply=%region_0.0 | reduce-window | flops 2080768 | bytes 131076 | tf_op jit(solution)/shard_map/reduce-window
  13.6 1.7 fusion
  18.6 27.2 %all_to_all.20 = bf16[1,8,96,512]{3,2,0,1:T(8,128)(2,1)} all-to-all(bf16[1,8,96,512]{3,2,0,1:T(8,128)(2,1)S(1)} %bitcast.116), channel_id=1, replica_groups=mesh['ep'=8,'tp'=4] {'ep'}, dimensions={1} | all-to-all | bytes 1572864 | tf_op jit(solution)/shard_map/all_to_all | solution.py:18
  45.8 24.1 %all_to_all.21 = bf16[1,8,96,512]{3,2,0,1:T(8,128)(2,1)} all-to-all(bf16[1,8,96,512]{3,2,0,1:T(8,128)(2,1)S(1)} %bitcast.115), channel_id=1, replica_groups=mesh['ep'=8,'tp'=4] {'ep'}, dimensions={1} | all-to-all | bytes 1572864 | tf_op jit(solution)/shard_map/all_to_all | solution.py:18
  69.9 18.7 %all-gather.3.cloned.1.call-done = bf16[1,768,2048]{2,1,0:T(8,128)(2,1)} async-done(((bf16[1,768,512]{2,1,0:T(8,128)(2,1)}), bf16[1,768,2048]{2,1,0:T(8,128)(2,1)}) %all-gather.3.cloned.1.call-update) | async-done | bytes 3145744 | tf_op jit(solution)/shard_map/all_gather | solution.py:22
  88.6 4.5 %fusion.7 = f32[768,512]{1,0:T(8,128)S(1)} fusion(bf16[1,768,2048]{2,1,0:T(8,128)(2,1)} %all-gather.3.cloned.1.call-done, bf16[2,2048,512]{2,1,0:T(8,128)(2,1)} %param.11), kind=kOutput, calls=%fused_computation.9 | convolution fusion | flops 1610612736 | bytes 6815744 | tf_op jit(solution)/shard_map/lrd,ldf->lrf/dot_general | solution.py:23
  93.3 2.1 multiply_convert_fusion.1
  97.0 51.7 %all-gather.5.cloned.1.call-done = bf16[1,768,2048]{2,1,0:T(8,128)(2,1)} async-done(((bf16[1,768,512]{2,1,0:T(8,128)(2,1)}), bf16[1,768,2048]{2,1,0:T(8,128)(2,1)}) %all-gather.5.cloned.1.call-update) | async-done | bytes 3145744 | tf_op jit(solution)/shard_map/all_gather | solution.py:22
  148.7 4.5 %fusion.3 = f32[768,512]{1,0:T(8,128)S(1)} fusion(bf16[1,768,2048]{2,1,0:T(8,128)(2,1)} %all-gather.5.cloned.1.call-done, bf16[2,2048,512]{2,1,0:T(8,128)(2,1)} %param.11), kind=kOutput, calls=%fused_computation.5 | convolution fusion | flops 1610612736 | bytes 6815744 | tf_op jit(solution)/shard_map/lrd,ldf->lrf/dot_general | solution.py:23
  154.7 2.1 multiply_convert_fusion
  158.7 15.0 %collective-permute-done.1 = bf16[1,768,512]{2,1,0:T(8,128)(2,1)S(1)} collective-permute-done((bf16[1,768,512]{2,1,0:T(8,128)(2,1)S(1)}, bf16[1,768,512]{2,1,0:T(8,128)(2,1)S(1)}, u32[]{:S(2)}, u32[]{:S(2)}) %collective-permute-start.1) | collective-permute-done | bytes 786464 | tf_op jit(solution)/shard_map/ppermute | solution.py:40
  173.7 2.4 collective-permute-start.2
  176.6 14.0 %collective-permute-done.3 = bf16[1,768,512]{2,1,0:T(8,128)(2,1)} collective-permute-done((bf16[1,768,512]{2,1,0:T(8,128)(2,1)S(1)}, bf16[1,768,512]{2,1,0:T(8,128)(2,1)}, u32[]{:S(2)}, u32[]{:S(2)}) %collective-permute-start.3) | collective-permute-done | bytes 786464 | tf_op jit(solution)/shard_map/ppermute | solution.py:40
  190.6 2.4 collective-permute-start.4
  194.1 13.2 %collective-permute-done.2 = bf16[1,768,512]{2,1,0:T(8,128)(2,1)S(1)} collective-permute-done((bf16[1,768,512]{2,1,0:T(8,128)(2,1)S(1)}, bf16[1,768,512]{2,1,0:T(8,128)(2,1)S(1)}, u32[]{:S(2)}, u32[]{:S(2)}) %collective-permute-start.2) | collective-permute-done | bytes 786464 | tf_op jit(solution)/shard_map/ppermute | solution.py:40
  208.8 4.6 %all-to-all-start.1 = ((bf16[1,8,96,512]{3,2,0,1:T(8,128)(2,1)}), bf16[1,8,96,512]{3,2,0,1:T(8,128)(2,1)S(1)}, u32[]{:S(2)}, u32[]{:S(2)}) async-start(bf16[1,8,96,512]{3,2,0,1:T(8,128)(2,1)} %bitcast.117), calls=%async_computation.1 | async-start | bytes 1572864 | tf_op jit(solution)/shard_map/all_to_all | solution.py:51
  213.4 9.6 %collective-permute-done.4 = bf16[1,768,512]{2,1,0:T(8,128)(2,1)} collective-permute-done((bf16[1,768,512]{2,1,0:T(8,128)(2,1)}, bf16[1,768,512]{2,1,0:T(8,128)(2,1)}, u32[]{:S(2)}, u32[]{:S(2)}) %collective-permute-start.4) | collective-permute-done | bytes 786464 | tf_op jit(solution)/shard_map/ppermute | solution.py:40
  223.0 2.4 collective-permute-start.5
  227.1 1.7 fusion.28
  230.5 11.6 %collective-permute-done.5 = bf16[1,768,512]{2,1,0:T(8,128)(2,1)S(1)} collective-permute-done((bf16[1,768,512]{2,1,0:T(8,128)(2,1)}, bf16[1,768,512]{2,1,0:T(8,128)(2,1)S(1)}, u32[]{:S(2)}, u32[]{:S(2)}) %collective-permute-start.5) | collective-permute-done | bytes 786464 | tf_op jit(solution)/shard_map/ppermute | solution.py:40
  243.6 4.7 %all-to-all-start.3 = ((bf16[1,8,96,512]{3,2,0,1:T(8,128)(2,1)}), bf16[1,8,96,512]{3,2,0,1:T(8,128)(2,1)S(1)}, u32[]{:S(2)}, u32[]{:S(2)}) async-start(bf16[1,8,96,512]{3,2,0,1:T(8,128)(2,1)} %bitcast.118), calls=%async_computation.3 | async-start | bytes 1572864 | tf_op jit(solution)/shard_map/all_to_all | solution.py:51
  248.7 20.6 %all-to-all-done.3 = bf16[1,8,96,512]{3,2,0,1:T(8,128)(2,1)S(1)} async-done(((bf16[1,8,96,512]{3,2,0,1:T(8,128)(2,1)}), bf16[1,8,96,512]{3,2,0,1:T(8,128)(2,1)S(1)}, u32[]{:S(2)}, u32[]{:S(2)}) %all-to-all-start.3) | async-done | bytes 786464 | tf_op jit(solution)/shard_map/all_to_all | solution.py:51
  269.5 4.0 %gather_fusion = bf16[1024,512]{1,0:T(8,128)(2,1)S(1)} fusion(bf16[1536,512]{1,0:T(8,128)(2,1)S(1)} %bitcast.112, s32[1024]{0:T(1024)S(1)} %broadcast_clamp_fusion), kind=kCustom, calls=%fused_computation | custom fusion | bytes 2101248 | tf_op jit(solution)/shard_map/gather | solution.py:101
  274.2 2.1 multiply_reduce_fusion
  (65 shorter events, 20.2 us)
Async XLA Ops:
  6.5 8.8 %copy-start.1 = (bf16[256,2048]{1,0:T(8,128)(2,1)S(1)}, bf16[256,2048]{1,0:T(8,128)(2,1)}, u32[]{:S(2)}) copy-start(bf16[256,2048]{1,0:T(8,128)(2,1)} %param.7) | copy-start | bytes 3145732
  6.5 82.1 %all-gather.3.cloned.1.call-start = ((), (), s32[]{:S(2)}) async-start(), calls=%async_computation.4 | async-start | bytes 3932160 | tf_op jit(solution)/shard_map/all_gather | solution.py:22
  45.8 102.9 %all-gather.5.cloned.1.call-start = ((), (), s32[]{:S(2)}) async-start(), calls=%async_computation.5 | async-start | bytes 3932160 | tf_op jit(solution)/shard_map/all_gather | solution.py:22
  88.6 4.5 %copy-start.6 = (bf16[2,2048,512]{2,1,0:T(8,128)(2,1)S(1)}, bf16[2,2048,512]{2,1,0:T(8,128)(2,1)}, u32[]{:S(2)}) copy-start(bf16[2,2048,512]{2,1,0:T(8,128)(2,1)} %param.12) | copy-start | bytes 12582916
  88.6 4.7 %copy-start.9 = (bf16[1,768,2048]{2,1,0:T(8,128)(2,1)S(1)}, bf16[1,768,2048]{2,1,0:T(8,128)(2,1)}, u32[]{:S(2)}) copy-start(bf16[1,768,2048]{2,1,0:T(8,128)(2,1)} %all-gather.3.cloned.1.call-done) | copy-start | bytes 9437188
  95.4 57.7 %copy-start.2 = (bf16[768,512]{1,0:T(8,128)(2,1)}, bf16[768,512]{1,0:T(8,128)(2,1)S(1)}, u32[]{:S(2)}) copy-start(bf16[768,512]{1,0:T(8,128)(2,1)S(1)} %multiply_convert_fusion.1) | copy-start | bytes 2359300
  95.5 57.7 %collective-permute-start = (bf16[1,768,512]{2,1,0:T(8,128)(2,1)S(1)}, bf16[1,768,512]{2,1,0:T(8,128)(2,1)S(1)}, u32[]{:S(2)}, u32[]{:S(2)}) collective-permute-start(bf16[1,768,512]{2,1,0:T(8,128)(2,1)S(1)} %bitcast.119), channel_id=1, source_target_pairs={{0,3},{1,0},{2,1},{3,2},{4,7},{5,4},{6,5},{7,6},{8,11},{9,8},{10,9... | collective-permute-start | bytes 2359304 | tf_op jit(solution)/shard_map/ppermute | solution.py:40
  148.7 6.0 %copy-start.7 = (bf16[2,2048,512]{2,1,0:T(8,128)(2,1)S(1)}, bf16[2,2048,512]{2,1,0:T(8,128)(2,1)}, u32[]{:S(2)}) copy-start(bf16[2,2048,512]{2,1,0:T(8,128)(2,1)} %param.12) | copy-start | bytes 12582916
  148.7 6.0 %copy-start.8 = (bf16[1,768,2048]{2,1,0:T(8,128)(2,1)S(1)}, bf16[1,768,2048]{2,1,0:T(8,128)(2,1)}, u32[]{:S(2)}) copy-start(bf16[1,768,2048]{2,1,0:T(8,128)(2,1)} %all-gather.5.cloned.1.call-done) | copy-start | bytes 9437188
  153.2 20.5 %collective-permute-start.1 = (bf16[1,768,512]{2,1,0:T(8,128)(2,1)S(1)}, bf16[1,768,512]{2,1,0:T(8,128)(2,1)S(1)}, u32[]{:S(2)}, u32[]{:S(2)}) collective-permute-start(bf16[1,768,512]{2,1,0:T(8,128)(2,1)S(1)} %collective-permute-done), channel_id=1, source_target_pairs={{0,3},{1,0},{2,1},{3,2},{4,7},{5,4},{6,5},{7,6},{8,11},{9,8},{10,9... | collective-permute-start | bytes 2359304 | tf_op jit(solution)/shard_map/ppermute | solution.py:40
  154.7 3.7 %copy-start = (bf16[2,2048,512]{2,1,0:T(8,128)(2,1)S(1)}, bf16[2,2048,512]{2,1,0:T(8,128)(2,1)}, u32[]{:S(2)}) copy-start(bf16[2,2048,512]{2,1,0:T(8,128)(2,1)} %param.13) | copy-start | bytes 12582916
  156.8 1.8 copy-start.4
  156.8 19.2 %copy-start.3 = (bf16[768,512]{1,0:T(8,128)(2,1)S(1)}, bf16[768,512]{1,0:T(8,128)(2,1)}, u32[]{:S(2)}) copy-start(bf16[768,512]{1,0:T(8,128)(2,1)} %copy-done.2) | copy-start | bytes 2359300
  156.8 33.8 %collective-permute-start.3 = (bf16[1,768,512]{2,1,0:T(8,128)(2,1)S(1)}, bf16[1,768,512]{2,1,0:T(8,128)(2,1)}, u32[]{:S(2)}, u32[]{:S(2)}) collective-permute-start(bf16[1,768,512]{2,1,0:T(8,128)(2,1)S(1)} %bitcast.120), channel_id=1, source_target_pairs={{0,3},{1,0},{2,1},{3,2},{4,7},{5,4},{6,5},{7,6},{8,11},{9,8},{10,9... | collective-permute-start | bytes 2359304 | tf_op jit(solution)/shard_map/ppermute | solution.py:40
  173.7 33.7 %collective-permute-start.2 = (bf16[1,768,512]{2,1,0:T(8,128)(2,1)S(1)}, bf16[1,768,512]{2,1,0:T(8,128)(2,1)S(1)}, u32[]{:S(2)}, u32[]{:S(2)}) collective-permute-start(bf16[1,768,512]{2,1,0:T(8,128)(2,1)S(1)} %collective-permute-done.1), channel_id=1, source_target_pairs={{0,3},{1,0},{2,1},{3,2},{4,7},{5,4},{6,5},{7,6},{8,11},{9,8},{10,9... | collective-permute-start | bytes 2359304 | tf_op jit(solution)/shard_map/ppermute | solution.py:40
  190.6 32.4 %collective-permute-start.4 = (bf16[1,768,512]{2,1,0:T(8,128)(2,1)}, bf16[1,768,512]{2,1,0:T(8,128)(2,1)}, u32[]{:S(2)}, u32[]{:S(2)}) collective-permute-start(bf16[1,768,512]{2,1,0:T(8,128)(2,1)} %collective-permute-done.3), channel_id=1, source_target_pairs={{0,3},{1,0},{2,1},{3,2},{4,7},{5,4},{6,5},{7,6},{8,11},{9,8},{10,9... | collective-permute-start | bytes 2359304 | tf_op jit(solution)/shard_map/ppermute | solution.py:40
  208.8 34.8 %all-to-all-start.1 = ((bf16[1,8,96,512]{3,2,0,1:T(8,128)(2,1)}), bf16[1,8,96,512]{3,2,0,1:T(8,128)(2,1)S(1)}, u32[]{:S(2)}, u32[]{:S(2)}) async-start(bf16[1,8,96,512]{3,2,0,1:T(8,128)(2,1)} %bitcast.117), calls=%async_computation.1 | async-start | bytes 1572864 | tf_op jit(solution)/shard_map/all_to_all | solution.py:51
  223.0 19.1 %collective-permute-start.5 = (bf16[1,768,512]{2,1,0:T(8,128)(2,1)}, bf16[1,768,512]{2,1,0:T(8,128)(2,1)S(1)}, u32[]{:S(2)}, u32[]{:S(2)}) collective-permute-start(bf16[1,768,512]{2,1,0:T(8,128)(2,1)} %collective-permute-done.4), channel_id=1, source_target_pairs={{0,3},{1,0},{2,1},{3,2},{4,7},{5,4},{6,5},{7,6},{8,11},{9,8},{10,9... | collective-permute-start | bytes 2359304 | tf_op jit(solution)/shard_map/ppermute | solution.py:40
  243.6 4.9 %copy-start.5 = (f32[256,4]{0,1:T(4,128)S(1)}, f32[256,4]{0,1:T(4,128)}, u32[]{:S(2)}) copy-start(f32[256,4]{0,1:T(4,128)} %param.10) | copy-start | bytes 12292
  243.6 25.7 %all-to-all-start.3 = ((bf16[1,8,96,512]{3,2,0,1:T(8,128)(2,1)}), bf16[1,8,96,512]{3,2,0,1:T(8,128)(2,1)S(1)}, u32[]{:S(2)}, u32[]{:S(2)}) async-start(bf16[1,8,96,512]{3,2,0,1:T(8,128)(2,1)} %bitcast.118), calls=%async_computation.3 | async-start | bytes 1572864 | tf_op jit(solution)/shard_map/all_to_all | solution.py:51
Sparse Core Ops, SparseCore 0:
  45.9 42.6 all-gather.2
  90.4 58.2 all-gather.4
